TPU v7x, 32 devices: a whole 2x2x4 slice. The times are simulated.
32 devices in a mesh: kv: 8 (over z, x), tp: 4 (over y, core).
Axes of the slice: x: 2, y: 2, z: 4, core: 2. Of those that a mesh axis runs over, the one named last changes fastest.
Arguments:
- hidden_rows: bfloat16 [28, 4096], P(None, ('kv', 'tp')), may hold values from -6 to 6
- first_gain: float32 [4096], P('kv'), may hold values from 0.1 to 1.9
- first_gate: bfloat16 [4096, 11264], P('kv', 'tp'), may hold values from -0.125 to 0.125
- first_up: bfloat16 [4096, 11264], P('kv', 'tp'), may hold values from -0.125 to 0.125
- first_down: bfloat16 [11264, 4096], P('tp', 'kv'), may hold values from -0.078125 to 0.078125
- mix_gain: float32 [4096], P('kv'), may hold values from 0.1 to 1.9
- query_weight: bfloat16 [4096, 2048], P('kv', 'tp'), may hold values from -0.09375 to 0.09375
- key_weight: bfloat16 [4096, 2048], P('kv', 'tp'), may hold values from -0.09375 to 0.09375
- value_weight: bfloat16 [4096, 2048], P('kv', 'tp'), may hold values from -0.09375 to 0.09375
- forget_weight: bfloat16 [4096, 16], P('kv'), may hold values from -0.09375 to 0.09375
- forget_bias: float32 [16], replicated, may hold values from -8 to 2
- out_weight: bfloat16 [2048, 4096], P('tp', 'kv'), may hold values from -0.5 to 0.5
- second_gain: float32 [4096], P('kv'), may hold values from 0.1 to 1.9
- second_gate: bfloat16 [4096, 11264], P('kv', 'tp'), may hold values from -0.125 to 0.125
- second_up: bfloat16 [4096, 11264], P('kv', 'tp'), may hold values from -0.125 to 0.125
- second_down: bfloat16 [11264, 4096], P('tp', 'kv'), may hold values from -0.078125 to 0.078125
- cache_keys: bfloat16 [28, 2048, 2048], P(None, 'kv', 'tp'), may hold values from -48 to 48
- cache_values: bfloat16 [28, 2048, 2048], P(None, 'kv', 'tp'), may hold values from -6 to 6
- cache_gates: float32 [28, 16, 2048], P(None, 'tp', 'kv'), may hold values from -1 to 0
- lengths: int32 [28], replicated, may hold values from 1 to 2048, 16384 in all
Outputs:
- out_rows: bfloat16 [28, 4096], P(None, ('kv', 'tp'))
Inputs may be any that keep to these rules, and one draw needn't show every extreme that they name: Sequence b uses cache positions 0 to lengths[b] - 1; some sequence uses all 2048.
All inputs are finite; a program needn't handle non-finite values.
Results may differ from a plain program's by a relative error of at most 0.014.
Values may be sent and summed in bfloat16 or wider, within the bound.
No kernel may reach another device: no remote copies, remote signals or barrier semaphores. Data moves between devices by JAX's collectives and lax.ppermute only.
A program may use at most 128 MiB of HBM per device.

v0:
```python
import jax
import jax.numpy as jnp
from jax import lax
from jax.sharding import PartitionSpec as P

D = 4096
HEAD_DIM = 128
EPS = 1e-06
FLOOR = -1e30


def entering(x, axis, combine, identity):
    devices, mine = (lax.axis_size(axis), lax.axis_index(axis))
    everything = lax.all_gather(x, axis)
    start = jnp.broadcast_to(jnp.asarray(identity, x.dtype), x.shape)

    def lap(k, before):
        reached = k < mine
        new = combine(before, everything[k])
        return jnp.where(reached, new, before)

    return lax.fori_loop(0, devices, lap, start)


def joined(value, axis, join):
    pieces = jax.tree.map(lambda part: lax.all_gather(part, axis), value)
    head = jax.tree.map(lambda part: part[0], pieces)
    tail = jax.tree.map(lambda part: part[1:], pieces)
    total, _ = lax.scan(lambda total, share: (join(total, share), None), head, tail)
    return total


def widen(shard):
    return lax.all_gather(shard, "tp", axis=1, tiled=True)


def scaled_rows(block, gain):
    block32 = block.astype(jnp.float32)
    scaled = (block32 * gain).astype(jnp.bfloat16)
    squares = jnp.sum(block32 * block32, axis=1, keepdims=True)
    return (scaled, squares)


def feed_forward(block, gain, w_gate, w_up, w_down):
    scaled, squares = scaled_rows(block, gain)
    gate = jnp.dot(scaled, w_gate, preferred_element_type=jnp.float32)
    up_act = jnp.dot(scaled, w_up, preferred_element_type=jnp.float32)
    gate, up_act, squares = lax.psum((gate, up_act, squares), "kv")
    rscale = lax.rsqrt(squares / D + EPS)
    hidden = (jax.nn.silu(gate * rscale) * (up_act * rscale)).astype(jnp.bfloat16)
    return jnp.dot(hidden, w_down, preferred_element_type=jnp.float32)


def join_parts(first, second):
    top_a, mass_a, summed_a = first
    top_b, mass_b, summed_b = second
    peak = jnp.maximum(top_a, top_b)
    part_a = jnp.exp(top_a - peak)
    part_b = jnp.exp(top_b - peak)
    return (
        peak,
        mass_a * part_a + mass_b * part_b,
        summed_a * part_a[:, :, None] + summed_b * part_b[:, :, None],
    )


def attention(
    block,
    gain,
    query_weight,
    key_weight,
    value_weight,
    forget_weight,
    forget_bias,
    out_weight,
    cache_keys,
    cache_values,
    cache_gates,
    lengths,
):
    scaled, squares = scaled_rows(block, gain)
    seqs = block.shape[0]
    heads_dev = query_weight.shape[1] // HEAD_DIM
    span = cache_keys.shape[1]
    places = lax.axis_index("kv") * span + jnp.arange(span, dtype=jnp.int32)
    live = places[None, None, :] < lengths[:, None, None]
    kept = jnp.where(live, cache_gates, 0.0)
    running = jnp.cumsum(kept, axis=2)
    local_total = running[:, :, -1:]
    lower = entering(local_total, "kv", jnp.add, jnp.zeros_like(local_total))
    part_query = jnp.dot(scaled, query_weight, preferred_element_type=jnp.float32)
    part_key = jnp.dot(scaled, key_weight, preferred_element_type=jnp.float32)
    part_value = jnp.dot(scaled, value_weight, preferred_element_type=jnp.float32)
    part_logit = jnp.dot(scaled, forget_weight, preferred_element_type=jnp.float32)
    part_query, part_key, part_value, part_logit, squares, grand = lax.psum(
        (part_query, part_key, part_value, part_logit, squares, local_total), "kv"
    )
    rscale = lax.rsqrt(squares / D + EPS)
    query = (part_query * rscale).astype(jnp.bfloat16).reshape(seqs, heads_dev, HEAD_DIM)
    fresh_key = (part_key * rscale).astype(jnp.bfloat16).reshape(seqs, heads_dev, HEAD_DIM)
    fresh_value = (part_value * rscale).astype(jnp.bfloat16).reshape(seqs, heads_dev, HEAD_DIM)
    first_head = lax.axis_index("tp") * heads_dev
    own_logit = lax.dynamic_slice_in_dim(part_logit, first_head, heads_dev, 1)
    own_bias = lax.dynamic_slice_in_dim(forget_bias, first_head, heads_dev, 0)
    fresh_gate = jax.nn.log_sigmoid(own_logit * rscale + own_bias)
    bias = fresh_gate[:, :, None] + (grand - lower - running)
    factor = HEAD_DIM ** (-0.5)
    keys = cache_keys.reshape(seqs, span, heads_dev, HEAD_DIM)
    values = cache_values.reshape(seqs, span, heads_dev, HEAD_DIM)
    scores = (
        jnp.einsum("bphd,bhd->bhp", keys, query, preferred_element_type=jnp.float32) * factor + bias
    )
    top = jnp.max(jnp.where(live, scores, FLOOR), axis=2)
    weights = jnp.where(live, jnp.exp(scores - top[:, :, None]), 0.0)
    mass = jnp.sum(weights, axis=2)
    summed = jnp.einsum(
        "bhp,bphd->bhd", weights.astype(jnp.bfloat16), values, preferred_element_type=jnp.float32
    )
    top, mass, summed = joined((top, mass, summed), "kv", join_parts)
    own = jnp.einsum("bhd,bhd->bh", query, fresh_key, preferred_element_type=jnp.float32) * factor
    peak = jnp.maximum(top, own)
    keep = jnp.exp(top - peak)
    fresh = jnp.exp(own - peak)
    attended = (
        (summed * keep[:, :, None] + fresh_value.astype(jnp.float32) * fresh[:, :, None])
        / (mass * keep + fresh)[:, :, None]
    ).astype(jnp.bfloat16)
    attended = attended.reshape(seqs, heads_dev * HEAD_DIM)
    return jnp.dot(attended, out_weight, preferred_element_type=jnp.float32)


def advance(shard, block, partial_value, weight):
    total = lax.psum(partial_value, "tp")
    return (shard, (block.astype(jnp.float32) + weight * total).astype(jnp.bfloat16))


def local(
    hidden_rows,
    first_gain,
    first_gate,
    first_up,
    first_down,
    mix_gain,
    query_weight,
    key_weight,
    value_weight,
    forget_weight,
    forget_bias,
    out_weight,
    second_gain,
    second_gate,
    second_up,
    second_down,
    cache_keys,
    cache_values,
    cache_gates,
    lengths,
):
    shard = hidden_rows
    block = widen(shard)
    partial_value = feed_forward(block, first_gain, first_gate, first_up, first_down)
    shard, block = advance(shard, block, partial_value, 0.5)
    partial_value = attention(
        block,
        mix_gain,
        query_weight,
        key_weight,
        value_weight,
        forget_weight,
        forget_bias,
        out_weight,
        cache_keys,
        cache_values,
        cache_gates,
        lengths,
    )
    shard, block = advance(shard, block, partial_value, 1.0)
    partial_value = feed_forward(block, second_gain, second_gate, second_up, second_down)
    shard, block = advance(shard, block, partial_value, 0.5)
    columns = hidden_rows.shape[1]
    return lax.dynamic_slice_in_dim(block, lax.axis_index("tp") * columns, columns, 1)


def solution(mesh):
    return jax.shard_map(
        local,
        mesh=mesh,
        in_specs=(
            P(None, ("kv", "tp")),
            P("kv"),
            P("kv", "tp"),
            P("kv", "tp"),
            P("tp", "kv"),
            P("kv"),
            P("kv", "tp"),
            P("kv", "tp"),
            P("kv", "tp"),
            P("kv", None),
            P(),
            P("tp", "kv"),
            P("kv"),
            P("kv", "tp"),
            P("kv", "tp"),
            P("tp", "kv"),
            P(None, "kv", "tp"),
            P(None, "kv", "tp"),
            P(None, "tp", "kv"),
            P(),
        ),
        out_specs=P(None, ("kv", "tp")),
        check_vma=False,
    )
```

profile of v0, /device:TPU:0, one launch (start us, length us, event | category | flops | bytes accessed | tf_op | source)
XLA Modules:
  0.0 400.4 jit_solution(7020302194779085242)
XLA Ops:
  6.5 6.5 %all_gather.27 = bf16[28,512]{1,0:T(8,128)(2,1)S(1)} all-gather(bf16[28,128]{1,0:T(8,128)(2,1)} %param.24), channel_id=1, replica_groups=mesh['kv'=8,'tp'=4] {'tp'}, dimensions={1}, use_global_device_ids=true | all-gather | bytes 35840 | tf_op jit(solution)/shard_map/all_gather | solution.py:34
  13.1 2.0 fusion.27
  15.1 1.3 fusion.29
  16.8 2.3 reduce-window.6
  20.8 31.5 %all-gather = f32[224,4,1]{1,2,0:T(1,128)S(1)} all-gather(f32[28,4,1]{1,2,0:T(1,128)S(1)} %copy.78), channel_id=2, replica_groups=mesh['kv'=8,'tp'=4] {'kv'}, dimensions={0}, use_global_device_ids=true | all-gather | bytes 4032 | tf_op jit(solution)/shard_map/all_gather | solution.py:14
  52.6 21.3 %psum.106 = f32[28,1]{0,1:T(1,128)S(1)} all-reduce(f32[28,1]{0,1:T(1,128)S(1)} %bitcast.89), channel_id=1, replica_groups=mesh['kv'=8,'tp'=4] {'kv'}, use_global_device_ids=true, to_apply=%region_2.0 | all-reduce | flops 28 | bytes 224 | tf_op jit(solution)/shard_map/psum | solution.py:48
  73.9 19.2 %all-reduce.11.cloned.1.call-done = (f32[28,2816]{1,0:T(8,128)}, f32[28,2816]{1,0:T(8,128)}) async-done(((f32[28,2816]{1,0:T(8,128)}, f32[28,2816]{1,0:T(8,128)}), (f32[28,2816]{1,0:T(8,128)}, f32[28,2816]{1,0:T(8,128)})) %all-reduce.11.cloned.1.call-update) | async-done | bytes 630800 | tf_op jit(solution)/shard_map/psum | solution.py:48
  93.1 2.7 fusion.6
  95.8 10.7 %psum.108 = f32[28,512]{1,0:T(8,128)S(1)} all-reduce(f32[28,512]{1,0:T(8,128)S(1)} %fusion.6), channel_id=1, replica_groups=mesh['kv'=8,'tp'=4] {'tp'}, use_global_device_ids=true, to_apply=%region_4.5 | all-reduce | flops 14336 | bytes 114688 | tf_op jit(solution)/shard_map/psum | solution.py:133
  107.2 0.7 fusion.35
  107.9 1.9 fusion.33
  109.8 1.9 fusion.31
  111.6 1.9 fusion.37
  114.0 10.4 %copy.97 = bf16[28,256,512]{1,2,0:T(8,128)(2,1)} copy(bf16[28,256,512]{2,1,0:T(8,128)(2,1)} %param.40) | data formatting | bytes 14680064 | tf_op jit(solution)/shard_map/reshape | solution.py:108
  124.5 60.4 %all-reduce.7.cloned.1.call-done = (f32[28,512]{1,0:T(8,128)}, f32[28,1]{0,1:T(1,128)}, f32[28,512]{1,0:T(8,128)}, f32[28,4,1]{0,1,2:T(4,128)}, f32[28,16]{0,1:T(8,128)}, /*index=5*/f32[28,512]{1,0:T(8,128)}) async-done(((f32[28,512]{1,0:T(8,128)}, f32[28,1]{0,1:T(1,128)}, f32[28,512]{1,0:T(8,128)}, f32[28,4,1]{0,1,2:T(4,128)}, f32[28,16]{0,1:T(8,128)}, /*index=5*/f32[28,512]{1,0:T(8,128)}), ...) | async-done | bytes 174400 | tf_op jit(solution)/shard_map/psum | solution.py:95
  185.5 1.0 multiply_convert_fusion.6
  186.6 0.8 fusion.44
  188.2 4.1 %fusion.54 = f32[28,4,1,256]{3,2,1,0:T(1,128)S(1)} fusion(bf16[28,4,128,1]{2,3,1,0:T(2,128)(2,1)S(1)} %reshape.110, bf16[28,256,4,128]{1,3,2,0:T(8,128)(2,1)} %bitcast.79), kind=kOutput, calls=%fused_computation.84 | convolution fusion | flops 7340032 | bytes 7483392 | tf_op jit(solution)/shard_map/bphd,bhd->bhp/dot_general | solution.py:111
  193.0 26.1 %all-gather.5 = f32[8,28,4]{1,2,0:T(4,128)S(1)} all-gather(f32[1,28,4]{1,2,0:T(4,128)S(1)} %bitcast.86), channel_id=4, replica_groups=mesh['kv'=8,'tp'=4] {'kv'}, dimensions={0}, use_global_device_ids=true | all-gather | bytes 4032 | tf_op jit(solution)/shard_map/all_gather | solution.py:26
  219.7 26.1 %all-gather.4 = f32[8,28,4]{1,2,0:T(4,128)S(1)} all-gather(f32[1,28,4]{1,2,0:T(4,128)S(1)} %bitcast.85), channel_id=3, replica_groups=mesh['kv'=8,'tp'=4] {'kv'}, dimensions={0}, use_global_device_ids=true | all-gather | bytes 4032 | tf_op jit(solution)/shard_map/all_gather | solution.py:26
  246.4 4.1 %fusion.3 = f32[28,4,1,128]{3,2,1,0:T(1,128)S(1)} fusion(bf16[28,4,256,1]{2,1,0,3:T(4,128)(2,1)S(1)} %get-tuple-element.207, bf16[28,256,512]{2,1,0:T(8,128)(2,1)} %param.41), kind=kOutput, calls=%fused_computation.10 | convolution fusion | flops 7340032 | bytes 7454720 | tf_op jit(solution)/shard_map/bhp,bphd->bhd/dot_general | solution.py:116
  250.6 31.3 %all-gather.3 = f32[224,4,128]{2,1,0:T(4,128)S(1)} all-gather(f32[28,4,128]{2,1,0:T(4,128)S(1)} %bitcast.84), channel_id=5, replica_groups=mesh['kv'=8,'tp'=4] {'kv'}, dimensions={0}, use_global_device_ids=true | all-gather | bytes 516096 | tf_op jit(solution)/shard_map/all_gather | solution.py:26
  282.2 7.9 %while.28 = (s32[]{:T(128)}, f32[28,4]{0,1:T(4,128)S(1)}, f32[28,4]{0,1:T(4,128)S(1)}, f32[28,4,128]{2,1,0:T(4,128)S(1)}, f32[7,28,4]{1,2,0:T(4,128)}, /*index=5...) while((s32[]{:T(128)}, f32[28,4]{0,1:T(4,128)S(1)}, f32[28,4]{0,1:T(4,128)S(1)}, ...), condition=%wide.region_17.18_spmd, body=%wide.region_16.17_spmd.sunk | while | flops 43682 | bytes 178405 | solution.py:29
  282.2 0.7 fusion.74
  290.6 1.2 fusion.55
  291.8 10.7 %psum.115 = f32[28,512]{1,0:T(8,128)S(1)} all-reduce(f32[28,512]{1,0:T(8,128)S(1)} %fusion.55), channel_id=1, replica_groups=mesh['kv'=8,'tp'=4] {'tp'}, use_global_device_ids=true, to_apply=%region_20.21 | all-reduce | flops 14336 | bytes 114688 | tf_op jit(solution)/shard_map/psum | solution.py:133
  302.6 3.3 fusion.40
  305.9 1.3 fusion.41
  307.3 17.5 %psum.117 = f32[28,1]{0,1:T(1,128)S(1)} all-reduce(f32[28,1]{0,1:T(1,128)S(1)} %bitcast.88), channel_id=1, replica_groups=mesh['kv'=8,'tp'=4] {'kv'}, use_global_device_ids=true, to_apply=%region_23.24 | all-reduce | flops 28 | bytes 224 | tf_op jit(solution)/shard_map/psum | solution.py:48
  324.8 55.1 %all-reduce.9.cloned.1.call-done = (f32[28,2816]{1,0:T(8,128)}, f32[28,2816]{1,0:T(8,128)}) async-done(((f32[28,2816]{1,0:T(8,128)}, f32[28,2816]{1,0:T(8,128)}), (f32[28,2816]{1,0:T(8,128)}, f32[28,2816]{1,0:T(8,128)})) %all-reduce.9.cloned.1.call-update) | async-done | bytes 630800 | tf_op jit(solution)/shard_map/psum | solution.py:48
  379.9 2.7 fusion.7
  382.6 10.7 %psum.119 = f32[28,512]{1,0:T(8,128)S(1)} all-reduce(f32[28,512]{1,0:T(8,128)S(1)} %fusion.7), channel_id=1, replica_groups=mesh['kv'=8,'tp'=4] {'tp'}, use_global_device_ids=true, to_apply=%region_25.26 | all-reduce | flops 14336 | bytes 114688 | tf_op jit(solution)/shard_map/psum | solution.py:133
  (121 shorter events, 15.6 us)
Async XLA Ops:
  6.5 6.5 %copy-start = (bf16[512,2816]{1,0:T(8,128)(2,1)S(1)}, bf16[512,2816]{1,0:T(8,128)(2,1)}, u32[]{:S(2)}) copy-start(bf16[512,2816]{1,0:T(8,128)(2,1)} %param.27) | copy-start | bytes 8650756
  6.5 8.6 %copy-start.6 = (f32[512]{0:T(512)S(1)}, f32[512]{0:T(512)}, u32[]{:S(2)}) copy-start(f32[512]{0:T(512)} %param.25) | copy-start | bytes 6148
  6.5 86.6 %all-reduce.11.cloned.1.call-start = ((), (), s32[]{:S(2)}) async-start(), calls=%async_computation.2 | async-start | bytes 1441792 | tf_op jit(solution)/shard_map/psum | solution.py:48
  6.5 8.6 %copy-start.1 = (bf16[512,2816]{1,0:T(8,128)(2,1)S(1)}, bf16[512,2816]{1,0:T(8,128)(2,1)}, u32[]{:S(2)}) copy-start(bf16[512,2816]{1,0:T(8,128)(2,1)} %param.26) | copy-start | bytes 8650756
  13.1 3.5 copy-start.8
  13.1 3.6 copy-start.3
  16.5 168.4 %all-reduce.7.cloned.1.call-start = ((), (), s32[]{:S(2)}) async-start(), calls=%async_computation | async-start | bytes 414720 | tf_op jit(solution)/shard_map/psum | solution.py:95
  16.8 90.4 %copy-start.4 = (f32[512]{0:T(512)S(1)}, f32[512]{0:T(512)}, u32[]{:S(2)}) copy-start(f32[512]{0:T(512)} %param.29) | copy-start | bytes 6148
  16.8 90.4 %copy-start.5 = (bf16[512,16]{0,1:T(8,128)(2,1)S(1)}, bf16[512,16]{0,1:T(8,128)(2,1)}, u32[]{:S(2)}) copy-start(bf16[512,16]{0,1:T(8,128)(2,1)} %param.33) | copy-start | bytes 49156
  113.5 266.4 %all-reduce.9.cloned.1.call-start = ((), (), s32[]{:S(2)}) async-start(), calls=%async_computation.1 | async-start | bytes 1441792 | tf_op jit(solution)/shard_map/psum | solution.py:48
  114.0 10.4 %copy-start.9 = (f32[16]{0:T(128)S(1)}, f32[16]{0:T(128)}, u32[]{:S(2)}) copy-start(f32[16]{0:T(128)} %param.34) | copy-start | bytes 196
  250.6 52.1 %copy-start.7 = (f32[512]{0:T(512)S(1)}, f32[512]{0:T(512)}, u32[]{:S(2)}) copy-start(f32[512]{0:T(512)} %param.36) | copy-start | bytes 6148
  302.5 3.4 copy-start.2
Sparse Core Ops, SparseCore 0:
  16.6 76.4 all-reduce.10
  113.6 71.1 all-reduce.6
  307.4 72.4 all-reduce.8
where the time goes:
time: 401 us; the launch traced here: 400 us
  blocking collectives  192 us (48%)
  waiting for transfers between devices  135 us (34%)
  matrix products  29.2 us (7%)
  local copies, waits for them, and re-layouts  15.8 us (4%)
  other arithmetic  14.4 us (4%)
  between operations  13.4 us (3%)
    all_gather x3, blocking collectives, joined(): pieces = jax.tree.map(lambda part: lax.all_gather(part, axis), value)  83.5 us
    psum x2, waiting for transfers between devices, feed_forward(): gate, up_act, squares = lax.psum((gate, up_act, squares), 'kv')  74.3 us
    psum x1, waiting for transfers between devices, attention(): lax.psum((part_query, part_key, part_value, part_logit, squares, local_to...  60.4 us
    psum x2, blocking collectives, feed_forward(): gate, up_act, squares = lax.psum((gate, up_act, squares), 'kv')  38.8 us
    psum x3, blocking collectives, advance(): total = lax.psum(partial_value, 'tp')  32 us
    all_gather x1, blocking collectives, entering(): everything = lax.all_gather(x, axis)  31.5 us
    reshape x1, local copies, waits for them, and re-layouts, attention(): keys = cache_keys.reshape(seqs, span, heads_dev, HEAD_DIM)  10.4 us
  transfers between devices with their start and end apart: 3, of which 3 were waited for; matrix products, arithmetic and copies ran while one was open for 4% of the time, Pallas kernels for 0%

commit v1 on v0

--- a/solution.py
+++ b/solution.py
@@ -130,7 +130,7 @@
 
 
 def advance(shard, block, partial_value, weight):
-    total = lax.psum(partial_value, "tp")
+    total = jnp.sum(lax.all_gather(partial_value, "tp"), axis=0)
     return (shard, (block.astype(jnp.float32) + weight * total).astype(jnp.bfloat16))
 
 

time: 401 us -> 386 us (0.963)
  blocking collectives: 192 us -> 178 us
    psum x3 -> x0, blocking collectives: 32 us -> none  [advance(): total = lax.psum(partial_value, 'tp')]
    all_gather x0 -> x3, blocking collectives: none -> 17.3 us  [advance(): total = jnp.sum(lax.all_gather(partial_value, 'tp'), axis=0)]
where the time goes in v1:
time: 386 us; the launch traced here: 385 us
  blocking collectives  178 us (46%)
  waiting for transfers between devices  134 us (35%)
  matrix products  29.2 us (8%)
  local copies, waits for them, and re-layouts  15.8 us (4%)
  other arithmetic  14.5 us (4%)
  between operations  13.4 us (3%)
    all_gather x3, blocking collectives, joined(): pieces = jax.tree.map(lambda part: lax.all_gather(part, axis), value)  83.5 us
    psum x2, waiting for transfers between devices, feed_forward(): gate, up_act, squares = lax.psum((gate, up_act, squares), 'kv')  73.8 us
    psum x1, waiting for transfers between devices, attention(): lax.psum((part_query, part_key, part_value, part_logit, squares, local_to...  60.1 us
    psum x2, blocking collectives, feed_forward(): gate, up_act, squares = lax.psum((gate, up_act, squares), 'kv')  39 us
    all_gather x1, blocking collectives, entering(): everything = lax.all_gather(x, axis)  31.5 us
    all_gather x3, blocking collectives, advance(): total = jnp.sum(lax.all_gather(partial_value, 'tp'), axis=0)  17.3 us
    reshape x1, local copies, waits for them, and re-layouts, attention(): keys = cache_keys.reshape(seqs, span, heads_dev, HEAD_DIM)  10.4 us
  transfers between devices with their start and end apart: 3, of which 3 were waited for; matrix products, arithmetic and copies ran while one was open for 4% of the time, Pallas kernels for 0%

profile of v1, /device:TPU:0, one launch (start us, length us, event | category | flops | bytes accessed | tf_op | source)
XLA Modules:
  0.0 385.1 jit_solution(10716950421049110579)
XLA Ops:
  6.5 6.5 %all_gather.45 = bf16[28,512]{1,0:T(8,128)(2,1)S(1)} all-gather(bf16[28,128]{1,0:T(8,128)(2,1)} %param.24), channel_id=1, replica_groups=mesh['kv'=8,'tp'=4] {'tp'}, dimensions={1}, use_global_device_ids=true | all-gather | bytes 35840 | tf_op jit(solution)/shard_map/all_gather | solution.py:34
  13.1 2.0 fusion.25
  15.1 1.3 fusion.27
  16.8 2.3 reduce-window.6
  20.8 31.5 %all-gather.1 = f32[224,4,1]{1,2,0:T(1,128)S(1)} all-gather(f32[28,4,1]{1,2,0:T(1,128)S(1)} %copy.78), channel_id=3, replica_groups=mesh['kv'=8,'tp'=4] {'kv'}, dimensions={0}, use_global_device_ids=true | all-gather | bytes 4032 | tf_op jit(solution)/shard_map/all_gather | solution.py:14
  52.6 21.3 %psum.85 = f32[28,1]{0,1:T(1,128)S(1)} all-reduce(f32[28,1]{0,1:T(1,128)S(1)} %bitcast.95), channel_id=1, replica_groups=mesh['kv'=8,'tp'=4] {'kv'}, use_global_device_ids=true, to_apply=%region_2.0 | all-reduce | flops 28 | bytes 224 | tf_op jit(solution)/shard_map/psum | solution.py:48
  73.9 19.2 %all-reduce.11.cloned.1.call-done = (f32[28,2816]{1,0:T(8,128)}, f32[28,2816]{1,0:T(8,128)}) async-done(((f32[28,2816]{1,0:T(8,128)}, f32[28,2816]{1,0:T(8,128)}), (f32[28,2816]{1,0:T(8,128)}, f32[28,2816]{1,0:T(8,128)})) %all-reduce.11.cloned.1.call-update) | async-done | bytes 630800 | tf_op jit(solution)/shard_map/psum | solution.py:48
  93.1 2.7 convolution_bitcast_fusion.1
  95.8 5.8 %all-gather.7 = f32[4,28,512]{2,1,0:T(8,128)S(1)} all-gather(f32[1,28,512]{2,1,0:T(8,128)S(1)} %convolution_bitcast_fusion.1), channel_id=2, replica_groups=mesh['kv'=8,'tp'=4] {'tp'}, dimensions={0}, use_global_device_ids=true | all-gather | bytes 286720 | tf_op jit(solution)/shard_map/all_gather | solution.py:133
  102.3 0.7 fusion.33
  103.1 1.9 fusion.31
  104.9 1.9 fusion.29
  106.8 1.9 fusion.35
  109.1 10.4 %copy.97 = bf16[28,256,512]{1,2,0:T(8,128)(2,1)} copy(bf16[28,256,512]{2,1,0:T(8,128)(2,1)} %param.40) | data formatting | bytes 14680064 | tf_op jit(solution)/shard_map/reshape | solution.py:108
  119.6 60.1 %all-reduce.7.cloned.1.call-done = (f32[28,512]{1,0:T(8,128)}, f32[28,1]{0,1:T(1,128)}, f32[28,512]{1,0:T(8,128)}, f32[28,4,1]{0,1,2:T(4,128)}, f32[28,16]{0,1:T(8,128)}, /*index=5*/f32[28,512]{1,0:T(8,128)}) async-done(((f32[28,512]{1,0:T(8,128)}, f32[28,1]{0,1:T(1,128)}, f32[28,512]{1,0:T(8,128)}, f32[28,4,1]{0,1,2:T(4,128)}, f32[28,16]{0,1:T(8,128)}, /*index=5*/f32[28,512]{1,0:T(8,128)}), ...) | async-done | bytes 174400 | tf_op jit(solution)/shard_map/psum | solution.py:95
  180.4 1.0 multiply_convert_fusion.6
  181.4 0.8 fusion.42
  183.1 4.1 %fusion.52 = f32[28,4,1,256]{3,2,1,0:T(1,128)S(1)} fusion(bf16[28,4,128,1]{2,3,1,0:T(2,128)(2,1)S(1)} %reshape.122, bf16[28,256,4,128]{1,3,2,0:T(8,128)(2,1)} %bitcast.85), kind=kOutput, calls=%fused_computation.85 | convolution fusion | flops 7340032 | bytes 7483392 | tf_op jit(solution)/shard_map/bphd,bhd->bhp/dot_general | solution.py:111
  187.8 26.1 %all-gather.9 = f32[8,28,4]{1,2,0:T(4,128)S(1)} all-gather(f32[1,28,4]{1,2,0:T(4,128)S(1)} %bitcast.92), channel_id=5, replica_groups=mesh['kv'=8,'tp'=4] {'kv'}, dimensions={0}, use_global_device_ids=true | all-gather | bytes 4032 | tf_op jit(solution)/shard_map/all_gather | solution.py:26
  214.6 26.1 %all-gather.8 = f32[8,28,4]{1,2,0:T(4,128)S(1)} all-gather(f32[1,28,4]{1,2,0:T(4,128)S(1)} %bitcast.91), channel_id=4, replica_groups=mesh['kv'=8,'tp'=4] {'kv'}, dimensions={0}, use_global_device_ids=true | all-gather | bytes 4032 | tf_op jit(solution)/shard_map/all_gather | solution.py:26
  241.3 4.1 %fusion.3 = f32[28,4,1,128]{3,2,1,0:T(1,128)S(1)} fusion(bf16[28,4,256,1]{2,1,0,3:T(4,128)(2,1)S(1)} %get-tuple-element.207, bf16[28,256,512]{2,1,0:T(8,128)(2,1)} %param.41), kind=kOutput, calls=%fused_computation.10 | convolution fusion | flops 7340032 | bytes 7454720 | tf_op jit(solution)/shard_map/bhp,bphd->bhd/dot_general | solution.py:116
  245.4 31.3 %all-gather.4 = f32[224,4,128]{2,1,0:T(4,128)S(1)} all-gather(f32[28,4,128]{2,1,0:T(4,128)S(1)} %bitcast.90), channel_id=6, replica_groups=mesh['kv'=8,'tp'=4] {'kv'}, dimensions={0}, use_global_device_ids=true | all-gather | bytes 516096 | tf_op jit(solution)/shard_map/all_gather | solution.py:26
  277.0 7.9 %while.28 = (s32[]{:T(128)}, f32[28,4]{0,1:T(4,128)S(1)}, f32[28,4]{0,1:T(4,128)S(1)}, f32[28,4,128]{2,1,0:T(4,128)S(1)}, f32[7,28,4]{1,2,0:T(4,128)}, /*index=5...) while((s32[]{:T(128)}, f32[28,4]{0,1:T(4,128)S(1)}, f32[28,4]{0,1:T(4,128)S(1)}, ...), condition=%wide.region_17.18_spmd, body=%wide.region_16.17_spmd.sunk | while | flops 43682 | bytes 178405 | solution.py:29
  277.0 0.7 fusion.71
  285.4 1.2 convolution_bitcast_fusion.2
  286.7 5.8 %all-gather.10 = f32[4,28,512]{2,1,0:T(8,128)S(1)} all-gather(f32[1,28,512]{2,1,0:T(8,128)S(1)} %convolution_bitcast_fusion.2), channel_id=7, replica_groups=mesh['kv'=8,'tp'=4] {'tp'}, dimensions={0}, use_global_device_ids=true | all-gather | bytes 286720 | tf_op jit(solution)/shard_map/all_gather | solution.py:133
  292.6 3.3 fusion.38
  295.9 1.3 fusion.39
  297.3 17.7 %psum.94 = f32[28,1]{0,1:T(1,128)S(1)} all-reduce(f32[28,1]{0,1:T(1,128)S(1)} %bitcast.94), channel_id=1, replica_groups=mesh['kv'=8,'tp'=4] {'kv'}, use_global_device_ids=true, to_apply=%region_23.24 | all-reduce | flops 28 | bytes 224 | tf_op jit(solution)/shard_map/psum | solution.py:48
  314.9 54.6 %all-reduce.9.cloned.1.call-done = (f32[28,2816]{1,0:T(8,128)}, f32[28,2816]{1,0:T(8,128)}) async-done(((f32[28,2816]{1,0:T(8,128)}, f32[28,2816]{1,0:T(8,128)}), (f32[28,2816]{1,0:T(8,128)}, f32[28,2816]{1,0:T(8,128)})) %all-reduce.9.cloned.1.call-update) | async-done | bytes 630800 | tf_op jit(solution)/shard_map/psum | solution.py:48
  369.5 2.7 convolution_bitcast_fusion
  372.2 5.8 %all-gather.11 = f32[4,28,512]{2,1,0:T(8,128)S(1)} all-gather(f32[1,28,512]{2,1,0:T(8,128)S(1)} %convolution_bitcast_fusion), channel_id=8, replica_groups=mesh['kv'=8,'tp'=4] {'tp'}, dimensions={0}, use_global_device_ids=true | all-gather | bytes 286720 | tf_op jit(solution)/shard_map/all_gather | solution.py:133
  (124 shorter events, 15.6 us)
Async XLA Ops:
  6.5 6.5 %copy-start = (bf16[512,2816]{1,0:T(8,128)(2,1)S(1)}, bf16[512,2816]{1,0:T(8,128)(2,1)}, u32[]{:S(2)}) copy-start(bf16[512,2816]{1,0:T(8,128)(2,1)} %param.27) | copy-start | bytes 8650756
  6.5 8.6 %copy-start.6 = (f32[512]{0:T(512)S(1)}, f32[512]{0:T(512)}, u32[]{:S(2)}) copy-start(f32[512]{0:T(512)} %param.25) | copy-start | bytes 6148
  6.5 86.6 %all-reduce.11.cloned.1.call-start = ((), (), s32[]{:S(2)}) async-start(), calls=%async_computation.2 | async-start | bytes 1441792 | tf_op jit(solution)/shard_map/psum | solution.py:48
  6.5 8.6 %copy-start.1 = (bf16[512,2816]{1,0:T(8,128)(2,1)S(1)}, bf16[512,2816]{1,0:T(8,128)(2,1)}, u32[]{:S(2)}) copy-start(bf16[512,2816]{1,0:T(8,128)(2,1)} %param.26) | copy-start | bytes 8650756
  13.1 3.5 copy-start.8
  13.1 3.6 copy-start.3
  16.5 163.2 %all-reduce.7.cloned.1.call-start = ((), (), s32[]{:S(2)}) async-start(), calls=%async_computation | async-start | bytes 414720 | tf_op jit(solution)/shard_map/psum | solution.py:95
  19.4 83.0 %copy-start.4 = (f32[512]{0:T(512)S(1)}, f32[512]{0:T(512)}, u32[]{:S(2)}) copy-start(f32[512]{0:T(512)} %param.29) | copy-start | bytes 6148
  19.4 83.0 %copy-start.5 = (bf16[512,16]{0,1:T(8,128)(2,1)S(1)}, bf16[512,16]{0,1:T(8,128)(2,1)}, u32[]{:S(2)}) copy-start(bf16[512,16]{0,1:T(8,128)(2,1)} %param.33) | copy-start | bytes 49156
  108.6 260.9 %all-reduce.9.cloned.1.call-start = ((), (), s32[]{:S(2)}) async-start(), calls=%async_computation.1 | async-start | bytes 1441792 | tf_op jit(solution)/shard_map/psum | solution.py:48
  109.1 10.4 %copy-start.9 = (f32[16]{0:T(128)S(1)}, f32[16]{0:T(128)}, u32[]{:S(2)}) copy-start(f32[16]{0:T(128)} %param.34) | copy-start | bytes 196
  245.4 47.2 %copy-start.7 = (f32[512]{0:T(512)S(1)}, f32[512]{0:T(512)}, u32[]{:S(2)}) copy-start(f32[512]{0:T(512)} %param.36) | copy-start | bytes 6148
  292.5 3.4 copy-start.2
Sparse Core Ops, SparseCore 0:
  16.6 76.4 all-reduce.10
  108.8 70.9 all-reduce.6
  297.4 72.0 all-reduce.8
